TPU v7x, 32 devices: a whole 2x2x4 slice. The times are simulated.
32 devices in a mesh: sp: 8 (over z, y), tp: 4 (over x, core).
Axes of the slice: x: 2, y: 2, z: 4, core: 2. Of those that a mesh axis runs over, the one named last changes fastest.
Arguments:
- query_first: bfloat16 [6144, 8, 128], P('sp', 'tp'), may hold values from -5.375 to 5.375
- key_first: bfloat16 [6144, 8, 128], P('sp', 'tp'), may hold values from -5.375 to 5.375
- value_first: bfloat16 [6144, 8, 128], P('sp', 'tp'), may hold values from -6 to 6
- query_second: bfloat16 [6144, 8, 256], P('sp', 'tp'), may hold values from -5.375 to 5.375
- key_second: bfloat16 [6144, 8, 256], P('sp', 'tp'), may hold values from -5.375 to 5.375
- value_second: bfloat16 [6144, 8, 128], P('sp', 'tp'), may hold values from -6 to 6
- mix_lambda: float32 [2, 8], P(None, 'tp'), may hold values from 0.3 to 0.8
- head_gain: float32 [2, 8, 128], P(None, 'tp'), may hold values from 0.1 to 1.9
- out_weight: bfloat16 [2, 8, 128, 2048], P(None, 'tp'), may hold values from -0.125 to 0.125
- residual: bfloat16 [6144, 2048], P(('sp', 'tp')), may hold values from -6 to 6
- norm_gain: float32 [2, 2048], replicated, may hold values from 0.1 to 1.9
- up_weight: bfloat16 [2048, 8192], P('sp', 'tp'), may hold values from -0.125 to 0.125
- down_weight: bfloat16 [8192, 2048], P('tp', 'sp'), may hold values from -0.0625 to 0.0625
Outputs:
- mixed: bfloat16 [6144, 2048], P(('sp', 'tp'))
All inputs are finite; a program needn't handle non-finite values.
Results may differ from a plain program's by a relative error of at most 0.02.
Values may be sent and summed in bfloat16 or wider, within the bound.
No kernel may reach another device: no remote copies, remote signals or barrier semaphores. Data moves between devices by JAX's collectives and lax.ppermute only.
A program may use at most 128 MiB of HBM per device.

v0:
```python
import functools
import math

import jax
import jax.numpy as jnp
from jax import lax
from jax.experimental import pallas as pl
from jax.experimental.pallas import tpu as pltpu
from jax.sharding import PartitionSpec as P

EPSILON = 1e-05
LOG2_E = math.log2(math.e)
AXES = ("sp", "tp")
QUERY_BLOCK = 256


def layer_norm(activations, scales):
    average = jnp.mean(activations, axis=-1, keepdims=True)
    centred = activations - average
    spread = jnp.mean(centred * centred, axis=-1, keepdims=True)
    return centred * lax.rsqrt(spread + EPSILON) * scales


def attend_body(*refs, pieces, first, last):
    scal_ref, mask_ref, gain_ref, low_ref, high_ref = refs[:5]
    piece_refs = refs[5 : 5 + 2 * pieces]
    state_ref = None if first else refs[5 + 2 * pieces]
    out_ref = refs[-1]
    rows = low_ref.shape[0]
    value_size = gain_ref.shape[1]
    queries = jnp.concatenate([low_ref[...], high_ref[...]], axis=1)
    maps = [queries * mask_ref[c : c + 1, :] for c in range(2)]
    scale = scal_ref[0]
    upper = lax.broadcasted_iota(jnp.int32, (rows, 128), 1) >= 64
    running = [None, None]
    if not first:
        for c in range(2):
            kept = state_ref[c * rows : (c + 1) * rows, value_size:]
            top = jnp.max(jnp.where(upper, -jnp.inf, kept), axis=-1, keepdims=True)
            total = jnp.max(jnp.where(upper, kept, -jnp.inf), axis=-1, keepdims=True)
            running[c] = (state_ref[c * rows : (c + 1) * rows, :value_size], total, top)

    def score(piece, c):
        packed, key_high = piece_refs[2 * piece : 2 * piece + 2]
        keys = jnp.concatenate([packed[:, : key_high.shape[1]], key_high[...]], axis=1)
        return lax.dot_general(
            maps[c], keys, (((1,), (1,)), ((), ())), preferred_element_type=jnp.float32
        )

    def absorb(piece, c, scores):
        packed, key_high = piece_refs[2 * piece : 2 * piece + 2]
        values = packed[:, key_high.shape[1] :]
        scores = scores * scale
        newest = jnp.max(scores, axis=-1, keepdims=True)
        if running[c] is not None:
            newest = jnp.maximum(running[c][2], newest)
        weights = jnp.exp2(scores - newest).astype(jnp.bfloat16)
        extended = jnp.concatenate([values, jnp.ones_like(values)], axis=1)
        summed = jnp.dot(weights, extended, preferred_element_type=jnp.float32)
        numerator, total = summed[:, :value_size], summed[:, value_size:]
        if running[c] is not None:
            factor = jnp.exp2(running[c][2] - newest)
            numerator = running[c][0] * factor + numerator
            total = running[c][1] * factor + total
        running[c] = (numerator, total, newest)

    items = [(piece, c) for piece in range(pieces) for c in range(2)]
    waiting = score(*items[0])
    for item, following in zip(items, items[1:] + [None]):
        ahead = score(*following) if following else None
        absorb(*item, waiting)
        waiting = ahead
    if last:
        ratio = [numerator / total for numerator, total, _ in running]
        attended = ratio[0] - scal_ref[1] * ratio[1]
        mean_square = jnp.mean(attended * attended, axis=-1, keepdims=True)
        scaled = attended * lax.rsqrt(mean_square + EPSILON) * gain_ref[...]
        out_ref[...] = scaled.astype(out_ref.dtype)
    else:
        for c, (numerator, total, top) in enumerate(running):
            out_ref[c * rows : (c + 1) * rows, :value_size] = numerator
            out_ref[c * rows : (c + 1) * rows, value_size:] = jnp.where(upper, total, top)


def attend(scalars, masks, gain, query_low, query_high, pieces, state, last):
    count, wide = query_low.shape
    value_size = gain.shape[1]
    flat = [array for piece in pieces for array in piece]
    length = sum(piece[1].shape[0] for piece in pieces)
    state_width = value_size + 128
    state_spec = pl.BlockSpec((2 * QUERY_BLOCK, state_width), lambda i: (i, 0))
    operands = [scalars, masks, gain, query_low, query_high, *flat]
    in_specs = [
        pl.BlockSpec(memory_space=pltpu.SMEM),
        pl.BlockSpec((2, 2 * wide), lambda i: (0, 0)),
        pl.BlockSpec((1, value_size), lambda i: (0, 0)),
        pl.BlockSpec((QUERY_BLOCK, wide), lambda i: (i, 0)),
        pl.BlockSpec((QUERY_BLOCK, wide), lambda i: (i, 0)),
        *(pl.BlockSpec(array.shape, lambda i: (0, 0)) for array in flat),
    ]
    if state is not None:
        operands.append(state)
        in_specs.append(state_spec)
    if last:
        out_spec = pl.BlockSpec((QUERY_BLOCK, value_size), lambda i: (i, 0))
        out_shape = jax.ShapeDtypeStruct((count, value_size), jnp.bfloat16)
    else:
        out_spec = state_spec
        out_shape = jax.ShapeDtypeStruct((2 * count, state_width), jnp.float32)
    return pl.pallas_call(
        functools.partial(attend_body, pieces=len(pieces), first=state is None, last=last),
        grid=(count // QUERY_BLOCK,),
        in_specs=in_specs,
        out_specs=out_spec,
        out_shape=out_shape,
        compiler_params=pltpu.CompilerParams(vmem_limit_bytes=40 * 1024 * 1024),
        cost_estimate=pl.CostEstimate(
            flops=8 * count * length * (2 * wide + value_size),
            bytes_accessed=2 * (count + length) * 3 * wide + 16 * count * state_width,
            transcendentals=2 * count * length,
        ),
        name="attend",
    )(*operands)


def project_body(order_ref, *refs, members, blocks):
    parts, weights = refs[:members], refs[members : 2 * members]
    residual_ref, gain_ref, normed_ref, half_ref, scratch_ref = refs[2 * members :]
    projected = residual_ref[...].astype(jnp.float32)
    for part, weight in zip(parts, weights):
        projected = projected + jnp.dot(part[...], weight[...], preferred_element_type=jnp.float32)
    normed = layer_norm(projected, gain_ref[...])
    column = normed.shape[1] // blocks
    for block in range(blocks):
        scratch_ref[block] = normed[:, block * column : (block + 1) * column]
    for block in range(blocks):
        moved = scratch_ref[order_ref[block]]
        normed_ref[:, block * column : (block + 1) * column] = moved
        half_ref[:, block * column : (block + 1) * column] = moved.astype(half_ref.dtype)


def project(order, parts, weights, residual, gain):
    rows, width = residual.shape
    blocks = order.shape[0]
    vmem = pl.BlockSpec(memory_space=pltpu.VMEM)
    return pl.pallas_call(
        functools.partial(project_body, members=len(parts), blocks=blocks),
        in_specs=[pl.BlockSpec(memory_space=pltpu.SMEM)] + [vmem] * (2 * len(parts) + 2),
        out_specs=(vmem, vmem),
        out_shape=(
            jax.ShapeDtypeStruct((rows, width), jnp.float32),
            jax.ShapeDtypeStruct((rows, width), jnp.bfloat16),
        ),
        scratch_shapes=[pltpu.VMEM((blocks, rows, width // blocks), jnp.float32)],
        compiler_params=pltpu.CompilerParams(vmem_limit_bytes=40 * 1024 * 1024),
        cost_estimate=pl.CostEstimate(
            flops=2 * rows * width * sum(w.shape[0] for w in weights),
            bytes_accessed=2 * width * sum(w.shape[0] for w in weights),
            transcendentals=0,
        ),
        name="project",
    )(order, *parts, *weights, residual, gain)


def expand_body(*refs, members):
    entered = jnp.concatenate([ref[...] for ref in refs[:members]], axis=0)
    weights = refs[members:-1]
    size = weights[0].shape[0]
    total = None
    for index, ref in enumerate(weights):
        part = jnp.dot(
            entered[:, index * size : (index + 1) * size],
            ref[...],
            preferred_element_type=jnp.float32,
        )
        total = part if total is None else total + part
    refs[-1][...] = jnp.square(jnp.maximum(total, 0.0)).astype(refs[-1].dtype)


def expand(members, weights, tile):
    rows, width = members[0].shape
    size, hidden = weights[0].shape
    count = rows * len(members)
    return pl.pallas_call(
        functools.partial(expand_body, members=len(members)),
        grid=(hidden // tile,),
        in_specs=[pl.BlockSpec((rows, width), lambda j: (0, 0)) for _ in members]
        + [pl.BlockSpec((size, tile), lambda j: (0, j)) for _ in weights],
        out_specs=pl.BlockSpec((count, tile), lambda j: (0, j)),
        out_shape=jax.ShapeDtypeStruct((count, hidden), jnp.bfloat16),
        compiler_params=pltpu.CompilerParams(vmem_limit_bytes=40 * 1024 * 1024),
        cost_estimate=pl.CostEstimate(
            flops=2 * count * width * hidden,
            bytes_accessed=2 * (count * width + width * hidden + count * hidden),
            transcendentals=0,
        ),
        name="expand",
    )(*members, *weights)


def contract_body(hidden_ref, *refs):
    out_ref = refs[-1]
    column = refs[0].shape[1]
    for index, ref in enumerate(refs[:-1]):
        part = jnp.dot(hidden_ref[...], ref[...], preferred_element_type=jnp.float32)
        out_ref[:, index * column : (index + 1) * column] = part.astype(out_ref.dtype)


def contract(hidden, weights, row_block):
    count, size = hidden.shape
    column = weights[0].shape[1]
    width = column * len(weights)
    return pl.pallas_call(
        contract_body,
        grid=(count // row_block,),
        in_specs=[pl.BlockSpec((row_block, size), lambda i: (i, 0))]
        + [pl.BlockSpec((size, column), lambda i: (0, 0)) for _ in weights],
        out_specs=pl.BlockSpec((row_block, width), lambda i: (i, 0)),
        out_shape=jax.ShapeDtypeStruct((count, width), jnp.bfloat16),
        compiler_params=pltpu.CompilerParams(vmem_limit_bytes=40 * 1024 * 1024),
        cost_estimate=pl.CostEstimate(
            flops=2 * count * size * width,
            bytes_accessed=2 * (count * size + size * width + count * width),
            transcendentals=0,
        ),
        name="contract",
    )(hidden, *weights)


def solution(mesh):
    n_sp, n_tp = mesh.shape["sp"], mesh.shape["tp"]

    def pairs(move):
        listed = []
        for s in range(n_sp):
            for t in range(n_tp):
                target = move(s, t)
                if target is not None:
                    listed.append((s * n_tp + t, target[0] * n_tp + target[1]))
        return listed

    def send(array, move):
        return lax.ppermute(array, AXES, pairs(move))

    def local(
        query_first,
        key_first,
        value_first,
        query_second,
        key_second,
        value_second,
        mix_lambda,
        head_gain,
        out_weight,
        residual,
        norm_gain,
        up_weight,
        down_weight,
    ):
        tok, heads, wide = query_first.shape
        size_first, size_second = wide // 2, query_second.shape[2] // 2
        value_size = value_first.shape[2]
        ways = 2 * heads
        stride = n_sp // ways
        sp, tp = lax.axis_index("sp"), lax.axis_index("tp")
        mine = sp // stride
        is_second = mine >= heads
        place, parity = sp // 2, tp % 2
        line = n_sp // 2

        def swap(s, t):
            return (s - s % 2 + t % 2, t - t % 2 + s % 2) if s % 2 != t % 2 else None

        def swapped(block):
            moved = send(block, swap)
            return jnp.where(sp % 2 == tp % 2, block, moved)

        def core(s, t):
            return (s, t ^ 1)

        def along(step, hops):
            def move(s, t):
                z = s // 2
                came = z if step > 0 else line - 1 - z
                inside = 0 <= z + step < line
                return (s + 2 * step, t) if inside and came >= hops else None

            return move

        def shifted(step):
            return lambda s, t: ((s + step * stride) % n_sp, t)

        def only_high(move):
            def moved(s, t):
                target = move(s, t)
                return target if target[0] // stride >= heads else None

            return moved

        def across(step):
            return lambda s, t: (s - s % stride + (s % stride + step) % stride, t)

        def pick(array, way):
            return lax.dynamic_index_in_dim(array, way, 0, keepdims=False)

        def by_head(array):
            return jnp.transpose(array, (1, 0, 2))

        up_block = swapped(up_weight)
        down_block = swapped(down_weight)

        query_both, key_both = by_head(query_second), by_head(key_second)
        query_main = jnp.concatenate([by_head(query_first), query_both[:, :, :wide]])
        key_main = jnp.concatenate([by_head(key_first), key_both[:, :, :wide]])
        value_main = jnp.concatenate([by_head(value_first), by_head(value_second)])
        query_high, key_high = query_both[:, :, wide:], key_both[:, :, wide:]

        ways_of = [(mine + step) % ways for step in range(ways)]
        uppers = [jnp.maximum(way - heads, 0) for way in ways_of]

        def own_high(array):
            part = pick(array, uppers[0])
            return jnp.where(is_second, part, jnp.zeros_like(part))

        lows, highs = [pick(query_main, mine)], [own_high(query_high)]
        for step in range(1, ways):
            lows.append(send(pick(query_main, ways_of[step]), shifted(step)))
            part = pick(query_high, uppers[step])
            highs.append(send(part, only_high(shifted(step))))
        pieces = []
        packed_rows = []
        for step in range(ways):
            packed = jnp.concatenate(
                [pick(key_main, ways_of[step]), pick(value_main, ways_of[step])], axis=1
            )
            if step == 0:
                upper = own_high(key_high)
            else:
                packed = send(packed, shifted(step))
                upper = send(pick(key_high, uppers[step]), only_high(shifted(step)))
            packed_rows.append((packed, upper))
        for packed, upper in packed_rows:
            group = [(packed, upper)]
            for other in range(1, stride):
                moved = send(packed, across(other))
                moved_high = send(upper, only_high(across(other)))
                group.append((moved, moved_high))
            pieces.append(group)

        chains = {"up": (up_block, [], []), "down": (down_block, [], [])}
        for hop in range(line - 1):
            for (block, rising, falling) in chains.values():
                ahead = rising[-1] if hop else block
                behind = falling[-1] if hop else block
                rising.append(send(ahead, along(1, hop)))
                falling.append(send(behind, along(-1, hop)))

        rises = place >= line // 2
        far = jnp.maximum(place, line - 1 - place)

        def arrived(kind):
            block, rising, falling = chains[kind]
            slots = [block]
            for k in range(line - 1):
                candidates = [(rising[k], falling[k])]
                candidates += [(falling[j], rising[j]) for j in range(k - line // 2 + 1)]
                if len(candidates) > 1:
                    candidates = lax.optimization_barrier(candidates)
                slot = jnp.where(rises, *candidates[0])
                for j, pair in enumerate(candidates[1:]):
                    slot = jnp.where(k - far == j, jnp.where(rises, *pair), slot)
                slots.append(slot)
            return [(part, send(part, core)) for part in slots]

        table = [[z] for z in range(line)]
        for z, row in enumerate(table):
            below, above = list(range(z - 1, -1, -1)), list(range(z + 1, line))
            row += below + above if z >= line // 2 else above + below
        inverse = [[row.index(z) for z in range(line)] for row in table]
        block_of = jnp.asarray(table, jnp.int32)[place]
        slot_of = jnp.asarray(inverse, jnp.int32)[place]

        lanes = jnp.arange(2 * wide)[None, :]
        half = jnp.where(is_second, wide, size_first)
        masks = jnp.concatenate([lanes < half, lanes >= half]).astype(jnp.bfloat16)
        scale = jnp.where(is_second, 1.0 / math.sqrt(size_second), 1.0 / math.sqrt(size_first))
        way_lambda = pick(mix_lambda.reshape(ways), mine)
        way_gain = pick(head_gain.reshape(ways, value_size), mine)[None, :]
        scalars = jnp.stack([scale * LOG2_E, way_lambda]).astype(jnp.float32)
        query_low, query_up = jnp.concatenate(lows), jnp.concatenate(highs)
        state = None
        for step in range(ways):
            state = attend(
                scalars, masks, way_gain, query_low, query_up, pieces[step], state, step == ways - 1
            )
        head_out = state

        rows = tok // n_tp
        weight_rows = out_weight.reshape(ways * value_size, out_weight.shape[-1])
        out_weights = [weight_rows]
        for bit in range(1, n_tp):
            flip = core if bit % 2 else lambda s, t, bit=bit: (s, t ^ bit)
            source = out_weights[bit - 1] if bit % 2 else weight_rows
            out_weights.append(send(source, flip))
        returned = []
        for step in range(ways):
            part = head_out[step * tok : (step + 1) * tok]
            returned.append(part if step == 0 else send(part, shifted(-step)))
        returned = jnp.stack(returned)
        ordered = jnp.concatenate([pick(returned, (w - mine) % ways) for w in range(ways)], axis=1)
        width = residual.shape[1]
        column = width // n_sp
        sides = (parity, 1 - parity)
        arrival = jnp.stack([2 * block_of[k] + y for k in range(line) for y in sides]).astype(jnp.int32)
        parts = []
        for bit in range(n_tp):
            part = lax.dynamic_slice_in_dim(ordered, (tp ^ bit) * rows, rows, 0)
            flip = lambda s, t, bit=bit: (s, t ^ bit)
            parts.append(send(part, flip) if bit else part)
        normed, own_rows = project(arrival, parts, out_weights, residual, norm_gain[0:1])
        gain_blocks = norm_gain[1].reshape(n_sp, column)
        last_gain = jnp.concatenate([pick(gain_blocks, arrival[k]) for k in range(n_sp)])[None, :]

        def member(code):
            return lambda s, t: (s ^ (code % 2), t ^ (2 * (code // 2)))

        members = [own_rows] + [send(own_rows, member(r)) for r in range(1, n_tp)]
        up_slots = [weight for pair in arrived("up") for weight in pair]
        hidden = expand(members, up_slots, 512)
        down_slots = arrived("down")
        sums = []
        for slots in (down_slots[:-1], down_slots[-1:]):
            share = contract(hidden, [weight for pair in slots for weight in pair], rows)
            summed = share[:rows].astype(jnp.float32)
            for r in range(1, n_tp):
                moved = send(share[r * rows : (r + 1) * rows], member(r))
                summed = summed + moved.astype(jnp.float32)
            sums.append(summed)
        mixed = layer_norm(normed + jnp.concatenate(sums, axis=1), last_gain).astype(jnp.bfloat16)
        mixed = mixed.reshape(rows, n_sp, column).swapaxes(0, 1)
        placed = [
            pick(mixed, 2 * slot_of[z] + (parity if y == 0 else 1 - parity))
            for z in range(line)
            for y in range(2)
        ]
        return jnp.concatenate(placed, axis=1)

    return jax.shard_map(
        local,
        mesh=mesh,
        in_specs=(
            P("sp", "tp", None),
            P("sp", "tp", None),
            P("sp", "tp", None),
            P("sp", "tp", None),
            P("sp", "tp", None),
            P("sp", "tp", None),
            P(None, "tp"),
            P(None, "tp", None),
            P(None, "tp", None, None),
            P(("sp", "tp"), None),
            P(),
            P("sp", "tp"),
            P("tp", "sp"),
        ),
        out_specs=P(("sp", "tp"), None),
        check_vma=False,
    )
```

profile of v0, /device:TPU:0, one launch (start us, length us, event | category | flops | bytes accessed | tf_op | source)
XLA Modules:
  0.0 462.5 jit_solution(7803084600157963673)
XLA Ops:
  3.5 5.1 %collective-permute-start.2 = (bf16[768,128]{1,0:T(8,128)(2,1)}, bf16[768,128]{1,0:T(8,128)(2,1)S(1)}, u32[]{:S(2)}, u32[]{:S(2)}) collective-permute-start(bf16[768,128]{1,0:T(8,128)(2,1)} %get-tuple-element.66), channel_id=1, source_target_pairs={{0,24},{1,25},{2,26},{3,27},{4,28},{5,29},{6,30},{7,31},{8,0},{9,1... | collective-permute-start | bytes 589832 | tf_op jit(solution)/shard_map/ppermute | solution.py:243
  10.5 5.4 %collective-permute-start.5 = (bf16[768,128]{1,0:T(8,128)(2,1)}, bf16[768,128]{1,0:T(8,128)(2,1)}, u32[]{:S(2)}, u32[]{:S(2)}) collective-permute-start(bf16[768,128]{1,0:T(8,128)(2,1)} %get-tuple-element.72), channel_id=1, source_target_pairs={{0,24},{1,25},{2,26},{3,27},{4,28},{5,29},{6,30},{7,31},{24,16},{2... | collective-permute-start | bytes 589832 | tf_op jit(solution)/shard_map/ppermute | solution.py:243
  34.6 32.0 %collective-permute-start.10 = (bf16[768,256]{1,0:T(8,128)(2,1)S(1)}, bf16[768,256]{1,0:T(8,128)(2,1)S(1)}, u32[]{:S(2)}, u32[]{:S(2)}) collective-permute-start(bf16[768,256]{1,0:T(8,128)(2,1)S(1)} %pad_maximum_fusion.5), channel_id=1, source_target_pairs={{0,16},{1,17},{2,18},{3,19},{4,20},{5,21},{6,22},{7,23},{8,24},{9,... | collective-permute-start | bytes 1179656 | tf_op jit(solution)/shard_map/ppermute | solution.py:243
  71.0 16.1 %attend.4.refs_9_ = f32[6144,256]{1,0:T(8,128)S(1)} custom-call(f32[2]{0:T(128)S(1)} %pad_maximum_fusion.8.refs_0_, bf16[2,256]{1,0:T(2,128)(2,1)S(1)} %add_convert_fusion.refs_1_, f32[1,128]{1,0:T(1,128)S(1)} %constant_dynamic-slice_fusion.21.refs_2_, bf16[3072,128]{1,0:T(8,128)(2,1)S(1)} %pad_maximum_fusion.refs_3_, ...), custom_call_target="tpu_custom_call" | custom-call | flops 14495514624 | bytes 16121856 | tf_op jit(solution)/shard_map/attend/pallas_call | solution.py:110
  89.6 4.7 %collective-permute-start.7 = (bf16[768,128]{1,0:T(8,128)(2,1)S(1)}, bf16[768,128]{1,0:T(8,128)(2,1)S(1)}, u32[]{:S(2)}, u32[]{:S(2)}) collective-permute-start(bf16[768,128]{1,0:T(8,128)(2,1)S(1)} %get-tuple-element.70), channel_id=1, source_target_pairs={{0,24},{1,25},{2,26},{3,27},{4,28},{5,29},{6,30},{7,31},{24,16},{2... | collective-permute-start | bytes 589832 | tf_op jit(solution)/shard_map/ppermute | solution.py:243
  96.8 17.0 %attend.5.refs_9_ = f32[6144,256]{1,0:T(8,128)S(1)} custom-call(f32[2]{0:T(128)S(1)} %pad_maximum_fusion.8.refs_0_, bf16[2,256]{1,0:T(2,128)(2,1)S(1)} %add_convert_fusion.refs_1_, f32[1,128]{1,0:T(1,128)S(1)} %constant_dynamic-slice_fusion.21.refs_2_, bf16[3072,128]{1,0:T(8,128)(2,1)S(1)} %pad_maximum_fusion.refs_3_, ...), custom_call_target="tpu_custom_call" | custom-call | flops 14495514624 | bytes 16121856 | tf_op jit(solution)/shard_map/attend/pallas_call | solution.py:110
  120.9 17.0 %attend.6.refs_9_ = f32[6144,256]{1,0:T(8,128)S(1)} custom-call(f32[2]{0:T(128)S(1)} %pad_maximum_fusion.8.refs_0_, bf16[2,256]{1,0:T(2,128)(2,1)S(1)} %add_convert_fusion.refs_1_, f32[1,128]{1,0:T(1,128)S(1)} %constant_dynamic-slice_fusion.21.refs_2_, bf16[3072,128]{1,0:T(8,128)(2,1)S(1)} %pad_maximum_fusion.refs_3_, ...), custom_call_target="tpu_custom_call" | custom-call | flops 14495514624 | bytes 16121856 | tf_op jit(solution)/shard_map/attend/pallas_call | solution.py:110
  141.5 18.0 %attend.7 = bf16[3072,128]{1,0:T(8,128)(2,1)S(1)} custom-call(f32[2]{0:T(128)S(1)} %pad_maximum_fusion.8.refs_0_, bf16[2,256]{1,0:T(2,128)(2,1)S(1)} %add_convert_fusion.refs_1_, f32[1,128]{1,0:T(1,128)S(1)} %constant_dynamic-slice_fusion.21.refs_2_, bf16[3072,128]{1,0:T(8,128)(2,1)S(1)} %pad_maximum_fusion.refs_3_, ...), custom_call_target="tpu_custom_call" | custom-call | flops 14495514624 | bytes 16121856 | tf_op jit(solution)/shard_map/attend/pallas_call | solution.py:110
  159.6 6.2 %collective-permute-start.21 = (bf16[768,128]{1,0:T(8,128)(2,1)S(1)}, bf16[768,128]{1,0:T(8,128)(2,1)S(1)}, u32[]{:S(2)}, u32[]{:S(2)}) collective-permute-start(bf16[768,128]{1,0:T(8,128)(2,1)S(1)} %get-tuple-element.49), channel_id=1, source_target_pairs={{0,16},{1,17},{2,18},{3,19},{4,20},{5,21},{6,22},{7,23},{8,24},{9,... | collective-permute-start | bytes 589832 | tf_op jit(solution)/shard_map/ppermute | solution.py:243
  165.9 5.3 %collective-permute-done.22 = bf16[768,128]{1,0:T(8,128)(2,1)S(1)} collective-permute-done((bf16[768,128]{1,0:T(8,128)(2,1)S(1)}, bf16[768,128]{1,0:T(8,128)(2,1)S(1)}, u32[]{:S(2)}, u32[]{:S(2)}) %collective-permute-start.22) | collective-permute-done | bytes 196640 | tf_op jit(solution)/shard_map/ppermute | solution.py:243
  172.7 5.3 %collective-permute-done.21 = bf16[768,128]{1,0:T(8,128)(2,1)S(1)} collective-permute-done((bf16[768,128]{1,0:T(8,128)(2,1)S(1)}, bf16[768,128]{1,0:T(8,128)(2,1)S(1)}, u32[]{:S(2)}, u32[]{:S(2)}) %collective-permute-start.21) | collective-permute-done | bytes 196640 | tf_op jit(solution)/shard_map/ppermute | solution.py:243
  190.2 29.5 %collective-permute-done.24.refs_2_ = bf16[192,512]{1,0:T(8,128)(2,1)S(1)} collective-permute-done((bf16[192,512]{1,0:T(8,128)(2,1)S(1)}, bf16[192,512]{1,0:T(8,128)(2,1)S(1)}, u32[]{:S(2)}, u32[]{:S(2)}) %collective-permute-start.24) | collective-permute-done | bytes 196640 | tf_op jit(solution)/shard_map/ppermute | solution.py:243
  222.1 4.8 %collective-permute-done.25.refs_3_ = bf16[192,512]{1,0:T(8,128)(2,1)S(1)} collective-permute-done((bf16[192,512]{1,0:T(8,128)(2,1)S(1)}, bf16[192,512]{1,0:T(8,128)(2,1)S(1)}, u32[]{:S(2)}, u32[]{:S(2)}) %collective-permute-start.25) | collective-permute-done | bytes 196640 | tf_op jit(solution)/shard_map/ppermute | solution.py:243
  242.6 9.6 %collective-permute-done.45 = bf16[2048,256]{1,0:T(8,128)(2,1)} collective-permute-done((bf16[2048,256]{1,0:T(8,128)(2,1)}, bf16[2048,256]{1,0:T(8,128)(2,1)}, u32[]{:S(2)}, u32[]{:S(2)}) %collective-permute-start.45) | collective-permute-done | bytes 1048608 | tf_op jit(solution)/shard_map/ppermute | solution.py:243
  252.9 5.2 %collective-permute-done.46 = bf16[2048,256]{1,0:T(8,128)(2,1)} collective-permute-done((bf16[2048,256]{1,0:T(8,128)(2,1)}, bf16[2048,256]{1,0:T(8,128)(2,1)}, u32[]{:S(2)}, u32[]{:S(2)}) %collective-permute-start.46) | collective-permute-done | bytes 1048608 | tf_op jit(solution)/shard_map/ppermute | solution.py:243
  265.9 14.7 %collective-permute-done.38 = bf16[256,2048]{1,0:T(8,128)(2,1)} collective-permute-done((bf16[256,2048]{1,0:T(8,128)(2,1)}, bf16[256,2048]{1,0:T(8,128)(2,1)}, u32[]{:S(2)}, u32[]{:S(2)}) %collective-permute-start.38) | collective-permute-done | bytes 1048608 | tf_op jit(solution)/shard_map/ppermute | solution.py:243
  284.0 19.0 %collective-permute-done.49 = bf16[2048,256]{1,0:T(8,128)(2,1)S(1)} collective-permute-done((bf16[2048,256]{1,0:T(8,128)(2,1)}, bf16[2048,256]{1,0:T(8,128)(2,1)S(1)}, u32[]{:S(2)}, u32[]{:S(2)}) %collective-permute-start.49) | collective-permute-done | bytes 1048608 | tf_op jit(solution)/shard_map/ppermute | solution.py:243
  306.7 18.8 %collective-permute-done.41 = bf16[256,2048]{1,0:T(8,128)(2,1)} collective-permute-done((bf16[256,2048]{1,0:T(8,128)(2,1)}, bf16[256,2048]{1,0:T(8,128)(2,1)}, u32[]{:S(2)}, u32[]{:S(2)}) %collective-permute-start.41) | collective-permute-done | bytes 1048608 | tf_op jit(solution)/shard_map/ppermute | solution.py:243
  333.5 13.7 %collective-permute-done.55 = bf16[2048,256]{1,0:T(8,128)(2,1)} collective-permute-done((bf16[2048,256]{1,0:T(8,128)(2,1)S(1)}, bf16[2048,256]{1,0:T(8,128)(2,1)}, u32[]{:S(2)}, u32[]{:S(2)}) %collective-permute-start.55) | collective-permute-done | bytes 1048608 | tf_op jit(solution)/shard_map/ppermute | solution.py:243
  358.2 9.4 %collective-permute-done.30.refs_2_ = bf16[192,2048]{1,0:T(8,128)(2,1)S(1)} collective-permute-done((bf16[192,2048]{1,0:T(8,128)(2,1)S(1)}, bf16[192,2048]{1,0:T(8,128)(2,1)S(1)}, u32[]{:S(2)}, u32[]{:S(2)}) %collective-permute-start.30) | collective-permute-done | bytes 786464 | tf_op jit(solution)/shard_map/ppermute | solution.py:243
  368.4 15.9 %collective-permute-done.31.refs_3_ = bf16[192,2048]{1,0:T(8,128)(2,1)S(1)} collective-permute-done((bf16[192,2048]{1,0:T(8,128)(2,1)S(1)}, bf16[192,2048]{1,0:T(8,128)(2,1)S(1)}, u32[]{:S(2)}, u32[]{:S(2)}) %collective-permute-start.31) | collective-permute-done | bytes 786464 | tf_op jit(solution)/shard_map/ppermute | solution.py:243
  398.5 9.6 %expand.1.hidden_ref = bf16[768,2048]{1,0:T(8,128)(2,1)} custom-call(bf16[192,2048]{1,0:T(8,128)(2,1)S(1)} %copy-done.23, bf16[192,2048]{1,0:T(8,128)(2,1)S(1)} %copy-done.25, bf16[192,2048]{1,0:T(8,128)(2,1)S(1)} %copy-done.27, bf16[192,2048]{1,0:T(8,128)(2,1)S(1)} %copy-done.29, bf16[256,2048]{1,0:T(8,128)(2,1)S(1)} %copy-done.6, ...), custom_call_target="tpu_custom_call" | custom-call | flops 6442450944 | bytes 14680064 | tf_op jit(solution)/shard_map/expand/pallas_call | solution.py:184
  413.8 8.6 %contract.2 = bf16[768,1536]{1,0:T(8,128)(2,1)S(1)} custom-call(bf16[768,2048]{1,0:T(8,128)(2,1)S(1)} %copy-done.2, bf16[2048,256]{1,0:T(8,128)(2,1)} %broadcast_select_fusion.2.refs_0_, bf16[2048,256]{1,0:T(8,128)(2,1)} %collective-permute-done.44.refs_1_, bf16[2048,256]{1,0:T(8,128)(2,1)} %broadcast_select_fusion.1.refs_2_, ...), custom_call_target="tpu_custom_call" | custom-call | flops 4831838208 | bytes 11796480 | tf_op jit(solution)/shard_map/contract/pallas_call | solution.py:213
  429.7 27.7 %collective-permute-done.58 = bf16[192,512]{1,0:T(8,128)(2,1)S(1)} collective-permute-done((bf16[192,512]{1,0:T(8,128)(2,1)S(1)}, bf16[192,512]{1,0:T(8,128)(2,1)S(1)}, u32[]{:S(2)}, u32[]{:S(2)}) %collective-permute-start.58) | collective-permute-done | bytes 196640 | tf_op jit(solution)/shard_map/ppermute | solution.py:243
  (262 shorter events, 138.0 us)
Async XLA Ops:
  25.6 43.0 %collective-permute-start.14 = (bf16[768,256]{1,0:T(8,128)(2,1)S(1)}, bf16[768,256]{1,0:T(8,128)(2,1)S(1)}, u32[]{:S(2)}, u32[]{:S(2)}) collective-permute-start(bf16[768,256]{1,0:T(8,128)(2,1)S(1)} %pad_maximum_fusion.6), channel_id=1, source_target_pairs={{0,8},{1,9},{2,10},{3,11},{4,12},{5,13},{6,14},{7,15},{8,16},{9,17... | collective-permute-start | bytes 1179656 | tf_op jit(solution)/shard_map/ppermute | solution.py:243
  25.6 43.7 %collective-permute-start.18 = (bf16[768,256]{1,0:T(8,128)(2,1)S(1)}, bf16[768,256]{1,0:T(8,128)(2,1)S(1)}, u32[]{:S(2)}, u32[]{:S(2)}) collective-permute-start(bf16[768,256]{1,0:T(8,128)(2,1)S(1)} %pad_maximum_fusion.7.refs_5_), channel_id=1, source_target_pairs={{0,4},{1,5},{2,6},{3,7},{4,0},{5,1},{6,2},{7,3},{8,12},{9,13},{10,... | collective-permute-start | bytes 1179656 | tf_op jit(solution)/shard_map/ppermute | solution.py:243
  28.2 89.8 %collective-permute-start.6 = (bf16[768,256]{1,0:T(8,128)(2,1)S(1)}, bf16[768,256]{1,0:T(8,128)(2,1)S(1)}, u32[]{:S(2)}, u32[]{:S(2)}) collective-permute-start(bf16[768,256]{1,0:T(8,128)(2,1)S(1)} %pad_maximum_fusion.4), channel_id=1, source_target_pairs={{0,24},{1,25},{2,26},{3,27},{4,28},{5,29},{6,30},{7,31},{8,0},{9,1... | collective-permute-start | bytes 1179656 | tf_op jit(solution)/shard_map/ppermute | solution.py:243
  34.6 59.8 %collective-permute-start.10 = (bf16[768,256]{1,0:T(8,128)(2,1)S(1)}, bf16[768,256]{1,0:T(8,128)(2,1)S(1)}, u32[]{:S(2)}, u32[]{:S(2)}) collective-permute-start(bf16[768,256]{1,0:T(8,128)(2,1)S(1)} %pad_maximum_fusion.5), channel_id=1, source_target_pairs={{0,16},{1,17},{2,18},{3,19},{4,20},{5,21},{6,22},{7,23},{8,24},{9,... | collective-permute-start | bytes 1179656 | tf_op jit(solution)/shard_map/ppermute | solution.py:243
  94.4 135.5 %collective-permute-start.26 = (bf16[512,2048]{1,0:T(8,128)(2,1)S(1)}, bf16[512,2048]{1,0:T(8,128)(2,1)}, u32[]{:S(2)}, u32[]{:S(2)}) collective-permute-start(bf16[512,2048]{1,0:T(8,128)(2,1)S(1)} %bitcast.131), channel_id=1, source_target_pairs={{0,1},{1,0},{2,3},{3,2},{4,5},{5,4},{6,7},{7,6},{8,9},{9,8},{10,11... | collective-permute-start | bytes 6291464 | tf_op jit(solution)/shard_map/ppermute | solution.py:243
  116.4 65.1 %collective-permute-start.32 = (bf16[256,2048]{1,0:T(8,128)(2,1)}, bf16[256,2048]{1,0:T(8,128)(2,1)}, u32[]{:S(2)}, u32[]{:S(2)}) collective-permute-start(bf16[256,2048]{1,0:T(8,128)(2,1)} %param.26), channel_id=1, source_target_pairs={{1,4},{3,6},{4,1},{6,3},{9,12},{11,14},{12,9},{14,11},{17,20},{19,... | collective-permute-start | bytes 3145736 | tf_op jit(solution)/shard_map/ppermute | solution.py:243
  171.2 71.3 %collective-permute-start.27 = (bf16[512,2048]{1,0:T(8,128)(2,1)S(1)}, bf16[512,2048]{1,0:T(8,128)(2,1)}, u32[]{:S(2)}, u32[]{:S(2)}) collective-permute-start(bf16[512,2048]{1,0:T(8,128)(2,1)S(1)} %bitcast.132), channel_id=1, source_target_pairs={{0,2},{1,3},{2,0},{3,1},{4,6},{5,7},{6,4},{7,5},{8,10},{9,11},{10,... | collective-permute-start | bytes 6291464 | tf_op jit(solution)/shard_map/ppermute | solution.py:243
  181.4 38.3 %collective-permute-start.24 = (bf16[192,512]{1,0:T(8,128)(2,1)S(1)}, bf16[192,512]{1,0:T(8,128)(2,1)S(1)}, u32[]{:S(2)}, u32[]{:S(2)}) collective-permute-start(bf16[192,512]{1,0:T(8,128)(2,1)S(1)} %get-tuple-element.40), channel_id=1, source_target_pairs={{0,2},{1,3},{2,0},{3,1},{4,6},{5,7},{6,4},{7,5},{8,10},{9,11},{10,... | collective-permute-start | bytes 589832 | tf_op jit(solution)/shard_map/ppermute | solution.py:243
  184.3 46.9 %collective-permute-start.34 = (bf16[256,2048]{1,0:T(8,128)(2,1)S(1)}, bf16[256,2048]{1,0:T(8,128)(2,1)}, u32[]{:S(2)}, u32[]{:S(2)}) collective-permute-start(bf16[256,2048]{1,0:T(8,128)(2,1)S(1)} %broadcast_select_fusion.5.refs_4_), channel_id=1, source_target_pairs={{0,8},{1,9},{2,10},{3,11},{4,12},{5,13},{6,14},{7,15},{8,16},{9,17... | collective-permute-start | bytes 3145736 | tf_op jit(solution)/shard_map/ppermute | solution.py:243
  188.9 44.0 %collective-permute-start.35 = (bf16[256,2048]{1,0:T(8,128)(2,1)S(1)}, bf16[256,2048]{1,0:T(8,128)(2,1)}, u32[]{:S(2)}, u32[]{:S(2)}) collective-permute-start(bf16[256,2048]{1,0:T(8,128)(2,1)S(1)} %broadcast_select_fusion.5.refs_4_), channel_id=1, source_target_pairs={{8,0},{9,1},{10,2},{11,3},{12,4},{13,5},{14,6},{15,7},{16,8},{17,9... | collective-permute-start | bytes 3145736 | tf_op jit(solution)/shard_map/ppermute | solution.py:243
  232.9 47.7 %collective-permute-start.38 = (bf16[256,2048]{1,0:T(8,128)(2,1)}, bf16[256,2048]{1,0:T(8,128)(2,1)}, u32[]{:S(2)}, u32[]{:S(2)}) collective-permute-start(bf16[256,2048]{1,0:T(8,128)(2,1)} %collective-permute-done.35), channel_id=1, source_target_pairs={{8,0},{9,1},{10,2},{11,3},{12,4},{13,5},{14,6},{15,7},{16,8},{17,9... | collective-permute-start | bytes 3145736 | tf_op jit(solution)/shard_map/ppermute | solution.py:243
  242.5 84.4 %collective-permute-start.28 = (bf16[512,2048]{1,0:T(8,128)(2,1)}, bf16[512,2048]{1,0:T(8,128)(2,1)S(1)}, u32[]{:S(2)}, u32[]{:S(2)}) collective-permute-start(bf16[512,2048]{1,0:T(8,128)(2,1)} %collective-permute-done.27.refs_6_), channel_id=1, source_target_pairs={{0,1},{1,0},{2,3},{3,2},{4,5},{5,4},{6,7},{7,6},{8,9},{9,8},{10,11... | collective-permute-start | bytes 6291464 | tf_op jit(solution)/shard_map/ppermute | solution.py:243
  258.1 44.8 %collective-permute-start.49 = (bf16[2048,256]{1,0:T(8,128)(2,1)}, bf16[2048,256]{1,0:T(8,128)(2,1)S(1)}, u32[]{:S(2)}, u32[]{:S(2)}) collective-permute-start(bf16[2048,256]{1,0:T(8,128)(2,1)} %collective-permute-done.46), channel_id=1, source_target_pairs={{8,0},{9,1},{10,2},{11,3},{12,4},{13,5},{14,6},{15,7},{16,8},{17,9... | collective-permute-start | bytes 3145736 | tf_op jit(solution)/shard_map/ppermute | solution.py:243
  265.1 41.5 %collective-permute-start.40 = (bf16[256,2048]{1,0:T(8,128)(2,1)}, bf16[256,2048]{1,0:T(8,128)(2,1)S(1)}, u32[]{:S(2)}, u32[]{:S(2)}) collective-permute-start(bf16[256,2048]{1,0:T(8,128)(2,1)} %collective-permute-done.37), channel_id=1, source_target_pairs={{16,24},{17,25},{18,26},{19,27},{20,28},{21,29},{22,30},{23,31}} | collective-permute-start | bytes 3145736 | tf_op jit(solution)/shard_map/ppermute | solution.py:243
  280.6 44.9 %collective-permute-start.41 = (bf16[256,2048]{1,0:T(8,128)(2,1)}, bf16[256,2048]{1,0:T(8,128)(2,1)}, u32[]{:S(2)}, u32[]{:S(2)}) collective-permute-start(bf16[256,2048]{1,0:T(8,128)(2,1)} %collective-permute-done.38), channel_id=1, source_target_pairs={{8,0},{9,1},{10,2},{11,3},{12,4},{13,5},{14,6},{15,7}} | collective-permute-start | bytes 3145736 | tf_op jit(solution)/shard_map/ppermute | solution.py:243
  283.2 48.9 %collective-permute-start.54 = (bf16[2048,256]{1,0:T(8,128)(2,1)S(1)}, bf16[2048,256]{1,0:T(8,128)(2,1)S(1)}, u32[]{:S(2)}, u32[]{:S(2)}) collective-permute-start(bf16[2048,256]{1,0:T(8,128)(2,1)S(1)} %collective-permute-done.48), channel_id=1, source_target_pairs={{16,24},{17,25},{18,26},{19,27},{20,28},{21,29},{22,30},{23,31}} | collective-permute-start | bytes 3145736 | tf_op jit(solution)/shard_map/ppermute | solution.py:243
  302.9 44.2 %collective-permute-start.55 = (bf16[2048,256]{1,0:T(8,128)(2,1)S(1)}, bf16[2048,256]{1,0:T(8,128)(2,1)}, u32[]{:S(2)}, u32[]{:S(2)}) collective-permute-start(bf16[2048,256]{1,0:T(8,128)(2,1)S(1)} %collective-permute-done.49), channel_id=1, source_target_pairs={{8,0},{9,1},{10,2},{11,3},{12,4},{13,5},{14,6},{15,7}} | collective-permute-start | bytes 3145736 | tf_op jit(solution)/shard_map/ppermute | solution.py:243
  306.6 43.4 %collective-permute-start.33 = (bf16[256,2048]{1,0:T(8,128)(2,1)S(1)}, bf16[256,2048]{1,0:T(8,128)(2,1)S(1)}, u32[]{:S(2)}, u32[]{:S(2)}) collective-permute-start(bf16[256,2048]{1,0:T(8,128)(2,1)S(1)} %broadcast_select_fusion.5.refs_4_), channel_id=1, source_target_pairs={{0,1},{1,0},{2,3},{3,2},{4,5},{5,4},{6,7},{7,6},{8,9},{9,8},{10,11... | collective-permute-start | bytes 3145736 | tf_op jit(solution)/shard_map/ppermute | solution.py:243
  350.0 34.3 %collective-permute-start.31 = (bf16[192,2048]{1,0:T(8,128)(2,1)S(1)}, bf16[192,2048]{1,0:T(8,128)(2,1)S(1)}, u32[]{:S(2)}, u32[]{:S(2)}) collective-permute-start(bf16[192,2048]{1,0:T(8,128)(2,1)S(1)} %get-tuple-element.16.refs_0_), channel_id=1, source_target_pairs={{0,6},{1,7},{2,4},{3,5},{4,2},{5,3},{6,0},{7,1},{8,14},{9,15},{10,... | collective-permute-start | bytes 2359304 | tf_op jit(solution)/shard_map/ppermute | solution.py:243
  353.3 34.4 %collective-permute-start.42 = (bf16[256,2048]{1,0:T(8,128)(2,1)}, bf16[256,2048]{1,0:T(8,128)(2,1)}, u32[]{:S(2)}, u32[]{:S(2)}) collective-permute-start(bf16[256,2048]{1,0:T(8,128)(2,1)} %select_select_fusion.1.refs_10_), channel_id=1, source_target_pairs={{0,1},{1,0},{2,3},{3,2},{4,5},{5,4},{6,7},{7,6},{8,9},{9,8},{10,11... | collective-permute-start | bytes 3145736 | tf_op jit(solution)/shard_map/ppermute | solution.py:243
  355.6 52.5 %collective-permute-start.56 = (bf16[2048,256]{1,0:T(8,128)(2,1)S(1)}, bf16[2048,256]{1,0:T(8,128)(2,1)}, u32[]{:S(2)}, u32[]{:S(2)}) collective-permute-start(bf16[2048,256]{1,0:T(8,128)(2,1)S(1)} %select_select_fusion.refs_0_), channel_id=1, source_target_pairs={{0,1},{1,0},{2,3},{3,2},{4,5},{5,4},{6,7},{7,6},{8,9},{9,8},{10,11... | collective-permute-start | bytes 3145736 | tf_op jit(solution)/shard_map/ppermute | solution.py:243
  357.8 55.9 %collective-permute-start.44 = (bf16[2048,256]{1,0:T(8,128)(2,1)}, bf16[2048,256]{1,0:T(8,128)(2,1)}, u32[]{:S(2)}, u32[]{:S(2)}) collective-permute-start(bf16[2048,256]{1,0:T(8,128)(2,1)} %broadcast_select_fusion.2.refs_0_), channel_id=1, source_target_pairs={{0,1},{1,0},{2,3},{3,2},{4,5},{5,4},{6,7},{7,6},{8,9},{9,8},{10,11... | collective-permute-start | bytes 3145736 | tf_op jit(solution)/shard_map/ppermute | solution.py:243
  368.4 45.3 %collective-permute-start.47 = (bf16[2048,256]{1,0:T(8,128)(2,1)}, bf16[2048,256]{1,0:T(8,128)(2,1)}, u32[]{:S(2)}, u32[]{:S(2)}) collective-permute-start(bf16[2048,256]{1,0:T(8,128)(2,1)} %broadcast_select_fusion.1.refs_2_), channel_id=1, source_target_pairs={{0,1},{1,0},{2,3},{3,2},{4,5},{5,4},{6,7},{7,6},{8,9},{9,8},{10,11... | collective-permute-start | bytes 3145736 | tf_op jit(solution)/shard_map/ppermute | solution.py:243
  422.6 34.9 %collective-permute-start.53 = (bf16[192,1536]{1,0:T(8,128)(2,1)S(1)}, bf16[192,1536]{1,0:T(8,128)(2,1)S(1)}, u32[]{:S(2)}, u32[]{:S(2)}) collective-permute-start(bf16[192,1536]{1,0:T(8,128)(2,1)S(1)} %get-tuple-element.26), channel_id=1, source_target_pairs={{0,6},{1,7},{2,4},{3,5},{4,2},{5,3},{6,0},{7,1},{8,14},{9,15},{10,... | collective-permute-start | bytes 1769480 | tf_op jit(solution)/shard_map/ppermute | solution.py:243
  (79 other events, 1265.4 us)
where the time goes:
time: 464 us; the launch traced here: 463 us
  waiting for transfers between devices  186 us (40%)
  starting transfers between devices  113 us (24%)
  Pallas kernels  94.7 us (20%)
  local copies, waits for them, and re-layouts  41.3 us (9%)
  other arithmetic  22.1 us (5%)
  between operations  5.94 us (1%)
    ppermute x60, waiting for transfers between devices, send(): return lax.ppermute(array, AXES, pairs(move))  186 us
    ppermute x60, starting transfers between devices, send(): return lax.ppermute(array, AXES, pairs(move))  113 us
    pallas_call x4, Pallas kernels, attend(): pl.pallas_call(functools.partial(attend_body, pieces=len(pieces), first=s...  68.1 us
    unnamed x105, local copies, waits for them, and re-layouts  31.1 us
    pallas_call x2, Pallas kernels, contract(): pl.pallas_call(contract_body, grid=(count // row_block,), in_specs=[pl.Bl...  12.2 us
    pallas_call x1, Pallas kernels, expand(): pl.pallas_call(functools.partial(expand_body, members=len(members)), grid...  9.62 us
  transfers between devices with their start and end apart: 60, of which 15 were waited for; matrix products, arithmetic and copies ran while one was open for 7% of the time, Pallas kernels for 20%

commit v1 on v0

--- a/solution.py
+++ b/solution.py
@@ -123,35 +123,28 @@
     )(*operands)
 
 
-def project_body(order_ref, *refs, members, blocks):
+def project_body(*refs, members):
     parts, weights = refs[:members], refs[members : 2 * members]
-    residual_ref, gain_ref, normed_ref, half_ref, scratch_ref = refs[2 * members :]
+    residual_ref, gain_ref, normed_ref, half_ref = refs[2 * members :]
     projected = residual_ref[...].astype(jnp.float32)
     for part, weight in zip(parts, weights):
         projected = projected + jnp.dot(part[...], weight[...], preferred_element_type=jnp.float32)
     normed = layer_norm(projected, gain_ref[...])
-    column = normed.shape[1] // blocks
-    for block in range(blocks):
-        scratch_ref[block] = normed[:, block * column : (block + 1) * column]
-    for block in range(blocks):
-        moved = scratch_ref[order_ref[block]]
-        normed_ref[:, block * column : (block + 1) * column] = moved
-        half_ref[:, block * column : (block + 1) * column] = moved.astype(half_ref.dtype)
-
-
-def project(order, parts, weights, residual, gain):
+    normed_ref[...] = normed
+    half_ref[...] = normed.astype(half_ref.dtype)
+
+
+def project(parts, weights, residual, gain):
     rows, width = residual.shape
-    blocks = order.shape[0]
     vmem = pl.BlockSpec(memory_space=pltpu.VMEM)
     return pl.pallas_call(
-        functools.partial(project_body, members=len(parts), blocks=blocks),
-        in_specs=[pl.BlockSpec(memory_space=pltpu.SMEM)] + [vmem] * (2 * len(parts) + 2),
+        functools.partial(project_body, members=len(parts)),
+        in_specs=[vmem] * (2 * len(parts) + 2),
         out_specs=(vmem, vmem),
         out_shape=(
             jax.ShapeDtypeStruct((rows, width), jnp.float32),
             jax.ShapeDtypeStruct((rows, width), jnp.bfloat16),
         ),
-        scratch_shapes=[pltpu.VMEM((blocks, rows, width // blocks), jnp.float32)],
         compiler_params=pltpu.CompilerParams(vmem_limit_bytes=40 * 1024 * 1024),
         cost_estimate=pl.CostEstimate(
             flops=2 * rows * width * sum(w.shape[0] for w in weights),
@@ -159,72 +152,76 @@
             transcendentals=0,
         ),
         name="project",
-    )(order, *parts, *weights, residual, gain)
-
-
-def expand_body(*refs, members):
-    entered = jnp.concatenate([ref[...] for ref in refs[:members]], axis=0)
-    weights = refs[members:-1]
-    size = weights[0].shape[0]
-    total = None
-    for index, ref in enumerate(weights):
-        part = jnp.dot(
-            entered[:, index * size : (index + 1) * size],
-            ref[...],
-            preferred_element_type=jnp.float32,
+    )(*parts, *weights, residual, gain)
+
+
+def feed_body(order_ref, *refs, members, pieces):
+    rows_refs, weights = refs[:members], refs[members : members + pieces]
+    out_ref, entered_ref, total_ref = refs[-3:]
+    step = pl.program_id(0)
+    size, tile = weights[0].shape[0] // 2, weights[0].shape[1]
+
+    @pl.when(step == 0)
+    def _():
+        entered = jnp.concatenate([ref[...] for ref in rows_refs], axis=0)
+        for block in range(pieces):
+            entered_ref[block] = entered[:, block * size : (block + 1) * size]
+        total_ref[...] = jnp.zeros_like(total_ref)
+
+    expanded = None
+    for i in range(0, pieces, 2):
+        left = jnp.concatenate([entered_ref[order_ref[i]], entered_ref[order_ref[i + 1]]], axis=1)
+        right = jnp.concatenate([weights[i][:size], weights[i + 1][:size]], axis=0)
+        part = jnp.dot(left, right, preferred_element_type=jnp.float32)
+        expanded = part if expanded is None else expanded + part
+    hidden = jnp.square(jnp.maximum(expanded, 0.0)).astype(jnp.bfloat16)
+    for i in range(0, pieces, 2):
+        right = jnp.concatenate(
+            [
+                jnp.concatenate([weights[j][size:, a : a + size] for a in range(0, tile, size)], axis=0)
+                for j in (i, i + 1)
+            ],
+            axis=1,
         )
-        total = part if total is None else total + part
-    refs[-1][...] = jnp.square(jnp.maximum(total, 0.0)).astype(refs[-1].dtype)
-
-
-def expand(members, weights, tile):
+        part = jnp.dot(hidden, right, preferred_element_type=jnp.float32)
+        total_ref[order_ref[i]] += part[:, :size]
+        total_ref[order_ref[i + 1]] += part[:, size:]
+
+    @pl.when(step == pl.num_programs(0) - 1)
+    def _():
+        for block in range(pieces):
+            out_ref[:, block * size : (block + 1) * size] = total_ref[block].astype(out_ref.dtype)
+
+
+def feed(order, members, weights, tile):
     rows, width = members[0].shape
-    size, hidden = weights[0].shape
+    size, hidden = weights[0].shape[0] // 2, weights[0].shape[1]
     count = rows * len(members)
+    pieces = len(weights)
     return pl.pallas_call(
-        functools.partial(expand_body, members=len(members)),
+        functools.partial(feed_body, members=len(members), pieces=pieces),
         grid=(hidden // tile,),
-        in_specs=[pl.BlockSpec((rows, width), lambda j: (0, 0)) for _ in members]
-        + [pl.BlockSpec((size, tile), lambda j: (0, j)) for _ in weights],
-        out_specs=pl.BlockSpec((count, tile), lambda j: (0, j)),
-        out_shape=jax.ShapeDtypeStruct((count, hidden), jnp.bfloat16),
+        in_specs=[pl.BlockSpec(memory_space=pltpu.SMEM)]
+        + [pl.BlockSpec((rows, width), lambda j: (0, 0)) for _ in members]
+        + [pl.BlockSpec((2 * size, tile), lambda j: (0, j)) for _ in weights],
+        out_specs=pl.BlockSpec((count, width), lambda j: (0, 0)),
+        out_shape=jax.ShapeDtypeStruct((count, width), jnp.bfloat16),
+        scratch_shapes=[
+            pltpu.VMEM((pieces, count, size), jnp.bfloat16),
+            pltpu.VMEM((pieces, count, size), jnp.float32),
+        ],
         compiler_params=pltpu.CompilerParams(vmem_limit_bytes=40 * 1024 * 1024),
         cost_estimate=pl.CostEstimate(
-            flops=2 * count * width * hidden,
-            bytes_accessed=2 * (count * width + width * hidden + count * hidden),
+            flops=4 * count * width * hidden,
+            bytes_accessed=4 * (count * width + width * hidden),
             transcendentals=0,
         ),
-        name="expand",
-    )(*members, *weights)
-
-
-def contract_body(hidden_ref, *refs):
-    out_ref = refs[-1]
-    column = refs[0].shape[1]
-    for index, ref in enumerate(refs[:-1]):
-        part = jnp.dot(hidden_ref[...], ref[...], preferred_element_type=jnp.float32)
-        out_ref[:, index * column : (index + 1) * column] = part.astype(out_ref.dtype)
-
-
-def contract(hidden, weights, row_block):
-    count, size = hidden.shape
-    column = weights[0].shape[1]
-    width = column * len(weights)
-    return pl.pallas_call(
-        contract_body,
-        grid=(count // row_block,),
-        in_specs=[pl.BlockSpec((row_block, size), lambda i: (i, 0))]
-        + [pl.BlockSpec((size, column), lambda i: (0, 0)) for _ in weights],
-        out_specs=pl.BlockSpec((row_block, width), lambda i: (i, 0)),
-        out_shape=jax.ShapeDtypeStruct((count, width), jnp.bfloat16),
-        compiler_params=pltpu.CompilerParams(vmem_limit_bytes=40 * 1024 * 1024),
-        cost_estimate=pl.CostEstimate(
-            flops=2 * count * size * width,
-            bytes_accessed=2 * (count * size + size * width + count * width),
-            transcendentals=0,
-        ),
-        name="contract",
-    )(hidden, *weights)
+        name="feed",
+    )(order, *members, *weights)
+
+
+def member_groups(n_tp):
+    return ([0], list(range(1, n_tp - 1)), [n_tp - 1])
 
 
 def solution(mesh):
@@ -268,24 +265,14 @@
         place, parity = sp // 2, tp % 2
         line = n_sp // 2
 
-        def swap(s, t):
-            return (s - s % 2 + t % 2, t - t % 2 + s % 2) if s % 2 != t % 2 else None
-
-        def swapped(block):
-            moved = send(block, swap)
-            return jnp.where(sp % 2 == tp % 2, block, moved)
-
         def core(s, t):
             return (s, t ^ 1)
 
-        def along(step, hops):
-            def move(s, t):
-                z = s // 2
-                came = z if step > 0 else line - 1 - z
-                inside = 0 <= z + step < line
-                return (s + 2 * step, t) if inside and came >= hops else None
-
-            return move
+        def along(step):
+            return lambda s, t: ((s + 2 * step) % n_sp, t)
+
+        def beside(s, t):
+            return (s ^ 1, t)
 
         def shifted(step):
             return lambda s, t: ((s + step * stride) % n_sp, t)
@@ -305,9 +292,6 @@
 
         def by_head(array):
             return jnp.transpose(array, (1, 0, 2))
-
-        up_block = swapped(up_weight)
-        down_block = swapped(down_weight)
 
         query_both, key_both = by_head(query_second), by_head(key_second)
         query_main = jnp.concatenate([by_head(query_first), query_both[:, :, :wide]])
@@ -347,38 +331,32 @@
                 group.append((moved, moved_high))
             pieces.append(group)
 
-        chains = {"up": (up_block, [], []), "down": (down_block, [], [])}
-        for hop in range(line - 1):
-            for (block, rising, falling) in chains.values():
-                ahead = rising[-1] if hop else block
-                behind = falling[-1] if hop else block
-                rising.append(send(ahead, along(1, hop)))
-                falling.append(send(behind, along(-1, hop)))
-
-        rises = place >= line // 2
-        far = jnp.maximum(place, line - 1 - place)
-
-        def arrived(kind):
-            block, rising, falling = chains[kind]
-            slots = [block]
-            for k in range(line - 1):
-                candidates = [(rising[k], falling[k])]
-                candidates += [(falling[j], rising[j]) for j in range(k - line // 2 + 1)]
-                if len(candidates) > 1:
-                    candidates = lax.optimization_barrier(candidates)
-                slot = jnp.where(rises, *candidates[0])
-                for j, pair in enumerate(candidates[1:]):
-                    slot = jnp.where(k - far == j, jnp.where(rises, *pair), slot)
-                slots.append(slot)
-            return [(part, send(part, core)) for part in slots]
-
-        table = [[z] for z in range(line)]
-        for z, row in enumerate(table):
-            below, above = list(range(z - 1, -1, -1)), list(range(z + 1, line))
-            row += below + above if z >= line // 2 else above + below
-        inverse = [[row.index(z) for z in range(line)] for row in table]
-        block_of = jnp.asarray(table, jnp.int32)[place]
-        slot_of = jnp.asarray(inverse, jnp.int32)[place]
+        size = up_weight.shape[0] // 2
+
+        def packed_half(half):
+            up = lax.dynamic_slice_in_dim(up_weight, half * size, size, 0)
+            down = lax.dynamic_slice_in_dim(down_weight, half * size, size, 1)
+            squares = [down[a : a + size] for a in range(0, down.shape[0], size)]
+            return jnp.concatenate([up, jnp.concatenate(squares, axis=1)], axis=0)
+
+        own_half, other_half = packed_half(parity), send(packed_half(1 - parity), core)
+        same = place % 2 == parity
+        even, odd = jnp.where(same, own_half, other_half), jnp.where(same, other_half, own_half)
+        weight_pieces = []
+        for step in range(line):
+            piece = even
+            if step:
+                piece = send(odd if step % 2 else even, along(step))
+            for part in (piece, send(piece, beside)):
+                weight_pieces += [part, send(part, core)]
+        piece_order = jnp.stack(
+            [
+                2 * (2 * lax.rem(place - step + line, line) + (y + sp) % 2) + (c + tp) % 2
+                for step in range(line)
+                for y in range(2)
+                for c in range(2)
+            ]
+        ).astype(jnp.int32)
 
         lanes = jnp.arange(2 * wide)[None, :]
         half = jnp.where(is_second, wide, size_first)
@@ -408,42 +386,27 @@
             returned.append(part if step == 0 else send(part, shifted(-step)))
         returned = jnp.stack(returned)
         ordered = jnp.concatenate([pick(returned, (w - mine) % ways) for w in range(ways)], axis=1)
-        width = residual.shape[1]
-        column = width // n_sp
-        sides = (parity, 1 - parity)
-        arrival = jnp.stack([2 * block_of[k] + y for k in range(line) for y in sides]).astype(jnp.int32)
         parts = []
         for bit in range(n_tp):
             part = lax.dynamic_slice_in_dim(ordered, (tp ^ bit) * rows, rows, 0)
             flip = lambda s, t, bit=bit: (s, t ^ bit)
             parts.append(send(part, flip) if bit else part)
-        normed, own_rows = project(arrival, parts, out_weights, residual, norm_gain[0:1])
-        gain_blocks = norm_gain[1].reshape(n_sp, column)
-        last_gain = jnp.concatenate([pick(gain_blocks, arrival[k]) for k in range(n_sp)])[None, :]
+        normed, own_rows = project(parts, out_weights, residual, norm_gain[0:1])
 
         def member(code):
-            return lambda s, t: (s ^ (code % 2), t ^ (2 * (code // 2)))
+            return lambda s, t: (s ^ (2 * (code % 2)), t ^ (2 * (code // 2)))
 
         members = [own_rows] + [send(own_rows, member(r)) for r in range(1, n_tp)]
-        up_slots = [weight for pair in arrived("up") for weight in pair]
-        hidden = expand(members, up_slots, 512)
-        down_slots = arrived("down")
-        sums = []
-        for slots in (down_slots[:-1], down_slots[-1:]):
-            share = contract(hidden, [weight for pair in slots for weight in pair], rows)
-            summed = share[:rows].astype(jnp.float32)
-            for r in range(1, n_tp):
-                moved = send(share[r * rows : (r + 1) * rows], member(r))
-                summed = summed + moved.astype(jnp.float32)
-            sums.append(summed)
-        mixed = layer_norm(normed + jnp.concatenate(sums, axis=1), last_gain).astype(jnp.bfloat16)
-        mixed = mixed.reshape(rows, n_sp, column).swapaxes(0, 1)
-        placed = [
-            pick(mixed, 2 * slot_of[z] + (parity if y == 0 else 1 - parity))
-            for z in range(line)
-            for y in range(2)
-        ]
-        return jnp.concatenate(placed, axis=1)
+        mixed_sum = None
+        for group in member_groups(n_tp):
+            shares = feed(piece_order, [members[r] for r in group], weight_pieces, 512)
+            for index, r in enumerate(group):
+                share = shares[index * rows : (index + 1) * rows]
+                if r:
+                    share = send(share, member(r))
+                share = share.astype(jnp.float32)
+                mixed_sum = share if mixed_sum is None else mixed_sum + share
+        return layer_norm(normed + mixed_sum, norm_gain[1]).astype(jnp.bfloat16)
 
     return jax.shard_map(
         local,

time: 464 us -> 472 us (1.017)
  waiting for transfers between devices: 186 us -> 210 us
  other arithmetic: 22.1 us -> 11.8 us
  Pallas kernels: 94.7 us -> 102 us
  starting transfers between devices: 113 us -> 107 us
  between operations: 5.94 us -> 0.71 us
    ppermute x60 -> x51, waiting for transfers between devices: 186 us -> 210 us  [send(): return lax.ppermute(array, AXES, pairs(move))]
    select_n x8 -> x1, other arithmetic: 15 us -> 0.41 us  [local(): jnp.where(same, other_half, own_half)]
    pallas_call x4, Pallas kernels: 26.5 us -> 34.5 us  [the longest x3 28.5 us: feed(): pl.pallas_call(functools.partial(feed_body, members=len(members), pieces=...]
    ppermute x60 -> x51, starting transfers between devices: 113 us -> 107 us  [send(): return lax.ppermute(array, AXES, pairs(move))]
    unnamed x105 -> x97, local copies, waits for them, and re-layouts: 31.1 us -> 34.3 us
  transfers between devices with their start and end apart: 60 -> 51, of which waited for: 15 -> 14; matrix products, arithmetic and copies ran while one was open for 7% -> 5% of each run, Pallas kernels for 20% -> 22%
where the time goes in v1:
time: 472 us; the launch traced here: 471 us
  waiting for transfers between devices  210 us (44%)
  starting transfers between devices  107 us (23%)
  Pallas kernels  102 us (22%)
  local copies, waits for them, and re-layouts  39.6 us (8%)
  other arithmetic  11.8 us (2%)
    ppermute x51, waiting for transfers between devices, send(): return lax.ppermute(array, AXES, pairs(move))  210 us
    ppermute x51, starting transfers between devices, send(): return lax.ppermute(array, AXES, pairs(move))  107 us
    pallas_call x4, Pallas kernels, attend(): pl.pallas_call(functools.partial(attend_body, pieces=len(pieces), first=s...  67.4 us
    unnamed x97, local copies, waits for them, and re-layouts  34.3 us
    pallas_call x3, Pallas kernels, feed(): pl.pallas_call(functools.partial(feed_body, members=len(members), pieces=...  28.5 us
  transfers between devices with their start and end apart: 51, of which 14 were waited for; matrix products, arithmetic and copies ran while one was open for 5% of the time, Pallas kernels for 22%

profile of v1, /device:TPU:0, one launch (start us, length us, event | category | flops | bytes accessed | tf_op | source)
XLA Modules:
  0.0 470.6 jit_solution(2376691491655117022)
XLA Ops:
  3.6 5.1 %collective-permute-start.2 = (bf16[768,128]{1,0:T(8,128)(2,1)}, bf16[768,128]{1,0:T(8,128)(2,1)}, u32[]{:S(2)}, u32[]{:S(2)}) collective-permute-start(bf16[768,128]{1,0:T(8,128)(2,1)} %get-tuple-element.74), channel_id=1, source_target_pairs={{0,24},{1,25},{2,26},{3,27},{4,28},{5,29},{6,30},{7,31},{8,0},{9,1... | collective-permute-start | bytes 589832 | tf_op jit(solution)/shard_map/ppermute | solution.py:240
  10.7 5.4 %collective-permute-start.5 = (bf16[768,128]{1,0:T(8,128)(2,1)}, bf16[768,128]{1,0:T(8,128)(2,1)}, u32[]{:S(2)}, u32[]{:S(2)}) collective-permute-start(bf16[768,128]{1,0:T(8,128)(2,1)} %get-tuple-element.80), channel_id=1, source_target_pairs={{0,24},{1,25},{2,26},{3,27},{4,28},{5,29},{6,30},{7,31},{24,16},{2... | collective-permute-start | bytes 589832 | tf_op jit(solution)/shard_map/ppermute | solution.py:240
  54.7 15.9 %collective-permute-start.10 = (bf16[768,256]{1,0:T(8,128)(2,1)S(1)}, bf16[768,256]{1,0:T(8,128)(2,1)S(1)}, u32[]{:S(2)}, u32[]{:S(2)}) collective-permute-start(bf16[768,256]{1,0:T(8,128)(2,1)S(1)} %pad_maximum_fusion.7), channel_id=1, source_target_pairs={{0,16},{1,17},{2,18},{3,19},{4,20},{5,21},{6,22},{7,23},{8,24},{9,... | collective-permute-start | bytes 1179656 | tf_op jit(solution)/shard_map/ppermute | solution.py:240
  74.8 16.0 %attend.4.refs_9_ = f32[6144,256]{1,0:T(8,128)S(1)} custom-call(f32[2]{0:T(128)S(1)} %pad_maximum_fusion.10.refs_0_, bf16[2,256]{1,0:T(2,128)(2,1)S(1)} %add_convert_fusion.refs_1_, f32[1,128]{1,0:T(1,128)S(1)} %constant_dynamic-slice_fusion.6.refs_2_, bf16[3072,128]{1,0:T(8,128)(2,1)S(1)} %pad_maximum_fusion.2.refs_3_, ...), custom_call_target="tpu_custom_call" | custom-call | flops 14495514624 | bytes 16121856 | tf_op jit(solution)/shard_map/attend/pallas_call | solution.py:110
  96.9 16.8 %attend.5.refs_9_ = f32[6144,256]{1,0:T(8,128)S(1)} custom-call(f32[2]{0:T(128)S(1)} %pad_maximum_fusion.10.refs_0_, bf16[2,256]{1,0:T(2,128)(2,1)S(1)} %add_convert_fusion.refs_1_, f32[1,128]{1,0:T(1,128)S(1)} %constant_dynamic-slice_fusion.6.refs_2_, bf16[3072,128]{1,0:T(8,128)(2,1)S(1)} %pad_maximum_fusion.2.refs_3_, ...), custom_call_target="tpu_custom_call" | custom-call | flops 14495514624 | bytes 16121856 | tf_op jit(solution)/shard_map/attend/pallas_call | solution.py:110
  116.3 16.8 %attend.6.refs_9_ = f32[6144,256]{1,0:T(8,128)S(1)} custom-call(f32[2]{0:T(128)S(1)} %pad_maximum_fusion.10.refs_0_, bf16[2,256]{1,0:T(2,128)(2,1)S(1)} %add_convert_fusion.refs_1_, f32[1,128]{1,0:T(1,128)S(1)} %constant_dynamic-slice_fusion.6.refs_2_, bf16[3072,128]{1,0:T(8,128)(2,1)S(1)} %pad_maximum_fusion.2.refs_3_, ...), custom_call_target="tpu_custom_call" | custom-call | flops 14495514624 | bytes 16121856 | tf_op jit(solution)/shard_map/attend/pallas_call | solution.py:110
  133.1 17.9 %attend.7 = bf16[3072,128]{1,0:T(8,128)(2,1)S(1)} custom-call(f32[2]{0:T(128)S(1)} %pad_maximum_fusion.10.refs_0_, bf16[2,256]{1,0:T(2,128)(2,1)S(1)} %add_convert_fusion.refs_1_, f32[1,128]{1,0:T(1,128)S(1)} %constant_dynamic-slice_fusion.6.refs_2_, bf16[3072,128]{1,0:T(8,128)(2,1)S(1)} %pad_maximum_fusion.2.refs_3_, ...), custom_call_target="tpu_custom_call" | custom-call | flops 14495514624 | bytes 16121856 | tf_op jit(solution)/shard_map/attend/pallas_call | solution.py:110
  154.4 10.8 %collective-permute-start.21 = (bf16[768,128]{1,0:T(8,128)(2,1)S(1)}, bf16[768,128]{1,0:T(8,128)(2,1)S(1)}, u32[]{:S(2)}, u32[]{:S(2)}) collective-permute-start(bf16[768,128]{1,0:T(8,128)(2,1)S(1)} %get-tuple-element.57), channel_id=1, source_target_pairs={{0,16},{1,17},{2,18},{3,19},{4,20},{5,21},{6,22},{7,23},{8,24},{9,... | collective-permute-start | bytes 589832 | tf_op jit(solution)/shard_map/ppermute | solution.py:240
  165.2 5.3 %collective-permute-done.22 = bf16[768,128]{1,0:T(8,128)(2,1)S(1)} collective-permute-done((bf16[768,128]{1,0:T(8,128)(2,1)S(1)}, bf16[768,128]{1,0:T(8,128)(2,1)S(1)}, u32[]{:S(2)}, u32[]{:S(2)}) %collective-permute-start.22) | collective-permute-done | bytes 196640 | tf_op jit(solution)/shard_map/ppermute | solution.py:240
  172.0 5.9 %collective-permute-done.21 = bf16[768,128]{1,0:T(8,128)(2,1)S(1)} collective-permute-done((bf16[768,128]{1,0:T(8,128)(2,1)S(1)}, bf16[768,128]{1,0:T(8,128)(2,1)S(1)}, u32[]{:S(2)}, u32[]{:S(2)}) %collective-permute-start.21) | collective-permute-done | bytes 196640 | tf_op jit(solution)/shard_map/ppermute | solution.py:240
  184.2 36.2 %collective-permute-done.24.refs_2_ = bf16[192,512]{1,0:T(8,128)(2,1)S(1)} collective-permute-done((bf16[192,512]{1,0:T(8,128)(2,1)S(1)}, bf16[192,512]{1,0:T(8,128)(2,1)S(1)}, u32[]{:S(2)}, u32[]{:S(2)}) %collective-permute-start.24) | collective-permute-done | bytes 196640 | tf_op jit(solution)/shard_map/ppermute | solution.py:240
  220.4 7.2 %collective-permute-done.25.refs_3_ = bf16[192,512]{1,0:T(8,128)(2,1)S(1)} collective-permute-done((bf16[192,512]{1,0:T(8,128)(2,1)S(1)}, bf16[192,512]{1,0:T(8,128)(2,1)S(1)}, u32[]{:S(2)}, u32[]{:S(2)}) %collective-permute-start.25) | collective-permute-done | bytes 196640 | tf_op jit(solution)/shard_map/ppermute | solution.py:240
  232.0 23.6 %collective-permute-done.33.refs_5_.refs_6_ = bf16[256,2048]{1,0:T(8,128)(2,1)S(1)} collective-permute-done((bf16[256,2048]{1,0:T(8,128)(2,1)S(1)}, bf16[256,2048]{1,0:T(8,128)(2,1)S(1)}, u32[]{:S(2)}, u32[]{:S(2)}) %collective-permute-start.33) | collective-permute-done | bytes 1048608 | tf_op jit(solution)/shard_map/ppermute | solution.py:240
  255.6 44.1 %collective-permute-done.37.refs_9_.refs_10_ = bf16[256,2048]{1,0:T(8,128)(2,1)S(1)} collective-permute-done((bf16[256,2048]{1,0:T(8,128)(2,1)S(1)}, bf16[256,2048]{1,0:T(8,128)(2,1)S(1)}, u32[]{:S(2)}, u32[]{:S(2)}) %collective-permute-start.37) | collective-permute-done | bytes 1048608 | tf_op jit(solution)/shard_map/ppermute | solution.py:240
  307.3 18.4 %collective-permute-done.35.refs_7_.refs_8_ = bf16[256,2048]{1,0:T(8,128)(2,1)S(1)} collective-permute-done((bf16[256,2048]{1,0:T(8,128)(2,1)S(1)}, bf16[256,2048]{1,0:T(8,128)(2,1)S(1)}, u32[]{:S(2)}, u32[]{:S(2)}) %collective-permute-start.35) | collective-permute-done | bytes 1048608 | tf_op jit(solution)/shard_map/ppermute | solution.py:240
  325.7 22.6 %collective-permute-done.39.refs_11_.refs_12_ = bf16[256,2048]{1,0:T(8,128)(2,1)} collective-permute-done((bf16[256,2048]{1,0:T(8,128)(2,1)S(1)}, bf16[256,2048]{1,0:T(8,128)(2,1)}, u32[]{:S(2)}, u32[]{:S(2)}) %collective-permute-start.39) | collective-permute-done | bytes 1048608 | tf_op jit(solution)/shard_map/ppermute | solution.py:240
  348.2 20.6 %collective-permute-done.43.refs_15_.refs_16_ = bf16[256,2048]{1,0:T(8,128)(2,1)} collective-permute-done((bf16[256,2048]{1,0:T(8,128)(2,1)S(1)}, bf16[256,2048]{1,0:T(8,128)(2,1)}, u32[]{:S(2)}, u32[]{:S(2)}) %collective-permute-start.43) | collective-permute-done | bytes 1048608 | tf_op jit(solution)/shard_map/ppermute | solution.py:240
  369.4 6.0 %project.1 = (f32[192,2048]{1,0:T(8,128)S(1)}, bf16[192,2048]{1,0:T(8,128)(2,1)}) custom-call(bf16[192,512]{1,0:T(8,128)(2,1)S(1)} %get-tuple-element.50.refs_0_, bf16[192,512]{1,0:T(8,128)(2,1)S(1)} %collective-permute-done.23.refs_1_, bf16[192,512]{1,0:T(8,128)(2,1)S(1)} %collective-permute-done.24.refs_2_, ...), custom_call_target="tpu_custom_call" | custom-call | flops 1610612736 | bytes 8388608 | tf_op jit(solution)/shard_map/project/pallas_call | solution.py:140
  377.6 18.0 %collective-permute-start.49 = (bf16[192,2048]{1,0:T(8,128)(2,1)}, bf16[192,2048]{1,0:T(8,128)(2,1)}, u32[]{:S(2)}, u32[]{:S(2)}) collective-permute-start(bf16[192,2048]{1,0:T(8,128)(2,1)} %get-tuple-element.8.refs_0_), channel_id=1, source_target_pairs={{0,10},{1,11},{2,8},{3,9},{4,14},{5,15},{6,12},{7,13},{8,2},{9,3},... | collective-permute-start | bytes 2359304 | tf_op jit(solution)/shard_map/ppermute | solution.py:240
  400.8 13.5 %collective-permute-done.49.refs_0_ = bf16[192,2048]{1,0:T(8,128)(2,1)} collective-permute-done((bf16[192,2048]{1,0:T(8,128)(2,1)}, bf16[192,2048]{1,0:T(8,128)(2,1)}, u32[]{:S(2)}, u32[]{:S(2)}) %collective-permute-start.49) | collective-permute-done | bytes 786464 | tf_op jit(solution)/shard_map/ppermute | solution.py:240
  422.9 7.8 %feed.5 = bf16[192,2048]{1,0:T(8,128)(2,1)S(1)} custom-call(s32[16]{0:T(128)S(1)} %stack.96.order_ref, bf16[192,2048]{1,0:T(8,128)(2,1)} %collective-permute-done.49.refs_0_, bf16[256,2048]{1,0:T(8,128)(2,1)S(1)} %get-tuple-element.12.refs_1_.refs_2_, bf16[256,2048]{1,0:T(8,128)(2,1)S(1)} %collective-permute-done.30.refs_2_.refs_3_, ...), custom_call_target="tpu_custom_call" | custom-call | flops 3221225472 | bytes 18350080 | tf_op jit(solution)/shard_map/feed/pallas_call | solution.py:201
  433.7 12.8 %feed.4 = bf16[384,2048]{1,0:T(8,128)(2,1)} custom-call(s32[16]{0:T(128)S(1)} %stack.96.order_ref, bf16[192,2048]{1,0:T(8,128)(2,1)} %collective-permute-done.45.refs_0_, bf16[192,2048]{1,0:T(8,128)(2,1)} %collective-permute-done.46.refs_1_, bf16[256,2048]{1,0:T(8,128)(2,1)S(1)} %get-tuple-element.12.refs_1_.refs_2_, ...), custom_call_target="tpu_custom_call" | custom-call | flops 6442450944 | bytes 19922944 | tf_op jit(solution)/shard_map/feed/pallas_call | solution.py:201
  451.4 7.8 %feed.3 = bf16[192,2048]{1,0:T(8,128)(2,1)S(1)} custom-call(s32[16]{0:T(128)S(1)} %stack.96.order_ref, bf16[192,2048]{1,0:T(8,128)(2,1)} %get-tuple-element.8.refs_0_, bf16[256,2048]{1,0:T(8,128)(2,1)S(1)} %get-tuple-element.12.refs_1_.refs_2_, bf16[256,2048]{1,0:T(8,128)(2,1)S(1)} %collective-permute-done.30.refs_2_.refs_3_, ...), custom_call_target="tpu_custom_call" | custom-call | flops 3221225472 | bytes 18350080 | tf_op jit(solution)/shard_map/feed/pallas_call | solution.py:201
  459.2 8.2 %collective-permute-done.48 = bf16[192,2048]{1,0:T(8,128)(2,1)S(1)} collective-permute-done((bf16[192,2048]{1,0:T(8,128)(2,1)S(1)}, bf16[192,2048]{1,0:T(8,128)(2,1)S(1)}, u32[]{:S(2)}, u32[]{:S(2)}) %collective-permute-start.48) | collective-permute-done | bytes 786464 | tf_op jit(solution)/shard_map/ppermute | solution.py:240
  (221 shorter events, 107.4 us)
Async XLA Ops:
  37.1 35.5 %collective-permute-start.14 = (bf16[768,256]{1,0:T(8,128)(2,1)S(1)}, bf16[768,256]{1,0:T(8,128)(2,1)S(1)}, u32[]{:S(2)}, u32[]{:S(2)}) collective-permute-start(bf16[768,256]{1,0:T(8,128)(2,1)S(1)} %pad_maximum_fusion.8), channel_id=1, source_target_pairs={{0,8},{1,9},{2,10},{3,11},{4,12},{5,13},{6,14},{7,15},{8,16},{9,17... | collective-permute-start | bytes 1179656 | tf_op jit(solution)/shard_map/ppermute | solution.py:240
  50.3 43.1 %collective-permute-start.6 = (bf16[768,256]{1,0:T(8,128)(2,1)S(1)}, bf16[768,256]{1,0:T(8,128)(2,1)S(1)}, u32[]{:S(2)}, u32[]{:S(2)}) collective-permute-start(bf16[768,256]{1,0:T(8,128)(2,1)S(1)} %pad_maximum_fusion.6), channel_id=1, source_target_pairs={{0,24},{1,25},{2,26},{3,27},{4,28},{5,29},{6,30},{7,31},{8,0},{9,1... | collective-permute-start | bytes 1179656 | tf_op jit(solution)/shard_map/ppermute | solution.py:240
  54.7 39.4 %collective-permute-start.10 = (bf16[768,256]{1,0:T(8,128)(2,1)S(1)}, bf16[768,256]{1,0:T(8,128)(2,1)S(1)}, u32[]{:S(2)}, u32[]{:S(2)}) collective-permute-start(bf16[768,256]{1,0:T(8,128)(2,1)S(1)} %pad_maximum_fusion.7), channel_id=1, source_target_pairs={{0,16},{1,17},{2,18},{3,19},{4,20},{5,21},{6,22},{7,23},{8,24},{9,... | collective-permute-start | bytes 1179656 | tf_op jit(solution)/shard_map/ppermute | solution.py:240
  93.4 84.8 %collective-permute-start.29 = (bf16[256,2048]{1,0:T(8,128)(2,1)}, bf16[256,2048]{1,0:T(8,128)(2,1)S(1)}, u32[]{:S(2)}, u32[]{:S(2)}) collective-permute-start(bf16[256,2048]{1,0:T(8,128)(2,1)} %pad_maximum_fusion.1), channel_id=1, source_target_pairs={{0,1},{1,0},{2,3},{3,2},{4,5},{5,4},{6,7},{7,6},{8,9},{9,8},{10,11... | collective-permute-start | bytes 3145736 | tf_op jit(solution)/shard_map/ppermute | solution.py:240
  93.4 39.6 %collective-permute-start.9 = (bf16[768,128]{1,0:T(8,128)(2,1)S(1)}, bf16[768,128]{1,0:T(8,128)(2,1)S(1)}, u32[]{:S(2)}, u32[]{:S(2)}) collective-permute-start(bf16[768,128]{1,0:T(8,128)(2,1)S(1)} %collective-permute-done.7.refs_6_), channel_id=1, source_target_pairs={{16,20},{17,21},{18,22},{19,23},{20,16},{21,17},{22,18},{23,19},{2... | collective-permute-start | bytes 589832 | tf_op jit(solution)/shard_map/ppermute | solution.py:240
  94.8 38.3 %collective-permute-start.8 = (bf16[768,256]{1,0:T(8,128)(2,1)S(1)}, bf16[768,256]{1,0:T(8,128)(2,1)S(1)}, u32[]{:S(2)}, u32[]{:S(2)}) collective-permute-start(bf16[768,256]{1,0:T(8,128)(2,1)S(1)} %collective-permute-done.6.refs_5_), channel_id=1, source_target_pairs={{0,4},{1,5},{2,6},{3,7},{4,0},{5,1},{6,2},{7,3},{8,12},{9,13},{10,... | collective-permute-start | bytes 1179656 | tf_op jit(solution)/shard_map/ppermute | solution.py:240
  165.2 62.4 %collective-permute-start.26 = (bf16[512,2048]{1,0:T(8,128)(2,1)}, bf16[512,2048]{1,0:T(8,128)(2,1)}, u32[]{:S(2)}, u32[]{:S(2)}) collective-permute-start(bf16[512,2048]{1,0:T(8,128)(2,1)} %bitcast.36.refs_4_), channel_id=1, source_target_pairs={{0,1},{1,0},{2,3},{3,2},{4,5},{5,4},{6,7},{7,6},{8,9},{9,8},{10,11... | collective-permute-start | bytes 6291464 | tf_op jit(solution)/shard_map/ppermute | solution.py:240
  170.5 60.5 %collective-permute-start.27 = (bf16[512,2048]{1,0:T(8,128)(2,1)}, bf16[512,2048]{1,0:T(8,128)(2,1)}, u32[]{:S(2)}, u32[]{:S(2)}) collective-permute-start(bf16[512,2048]{1,0:T(8,128)(2,1)} %bitcast.36.refs_4_), channel_id=1, source_target_pairs={{0,2},{1,3},{2,0},{3,1},{4,6},{5,7},{6,4},{7,5},{8,10},{9,11},{10,... | collective-permute-start | bytes 6291464 | tf_op jit(solution)/shard_map/ppermute | solution.py:240
  179.5 52.0 %collective-permute-start.30 = (bf16[256,2048]{1,0:T(8,128)(2,1)S(1)}, bf16[256,2048]{1,0:T(8,128)(2,1)S(1)}, u32[]{:S(2)}, u32[]{:S(2)}) collective-permute-start(bf16[256,2048]{1,0:T(8,128)(2,1)S(1)} %get-tuple-element.12.refs_1_.refs_2_), channel_id=1, source_target_pairs={{0,1},{1,0},{2,3},{3,2},{4,5},{5,4},{6,7},{7,6},{8,9},{9,8},{10,11... | collective-permute-start | bytes 3145736 | tf_op jit(solution)/shard_map/ppermute | solution.py:240
  179.5 51.9 %collective-permute-start.31 = (bf16[256,2048]{1,0:T(8,128)(2,1)S(1)}, bf16[256,2048]{1,0:T(8,128)(2,1)S(1)}, u32[]{:S(2)}, u32[]{:S(2)}) collective-permute-start(bf16[256,2048]{1,0:T(8,128)(2,1)S(1)} %get-tuple-element.12.refs_1_.refs_2_), channel_id=1, source_target_pairs={{0,4},{1,5},{2,6},{3,7},{4,0},{5,1},{6,2},{7,3},{8,12},{9,13},{10,... | collective-permute-start | bytes 3145736 | tf_op jit(solution)/shard_map/ppermute | solution.py:240
  182.7 37.7 %collective-permute-start.24 = (bf16[192,512]{1,0:T(8,128)(2,1)S(1)}, bf16[192,512]{1,0:T(8,128)(2,1)S(1)}, u32[]{:S(2)}, u32[]{:S(2)}) collective-permute-start(bf16[192,512]{1,0:T(8,128)(2,1)S(1)} %get-tuple-element.48), channel_id=1, source_target_pairs={{0,2},{1,3},{2,0},{3,1},{4,6},{5,7},{6,4},{7,5},{8,10},{9,11},{10,... | collective-permute-start | bytes 589832 | tf_op jit(solution)/shard_map/ppermute | solution.py:240
  227.6 72.1 %collective-permute-start.37 = (bf16[256,2048]{1,0:T(8,128)(2,1)S(1)}, bf16[256,2048]{1,0:T(8,128)(2,1)S(1)}, u32[]{:S(2)}, u32[]{:S(2)}) collective-permute-start(bf16[256,2048]{1,0:T(8,128)(2,1)S(1)} %get-tuple-element.12.refs_1_.refs_2_), channel_id=1, source_target_pairs={{0,16},{1,17},{2,18},{3,19},{4,20},{5,21},{6,22},{7,23},{8,24},{9,... | collective-permute-start | bytes 3145736 | tf_op jit(solution)/shard_map/ppermute | solution.py:240
  231.0 71.2 %collective-permute-start.41 = (bf16[256,2048]{1,0:T(8,128)(2,1)S(1)}, bf16[256,2048]{1,0:T(8,128)(2,1)S(1)}, u32[]{:S(2)}, u32[]{:S(2)}) collective-permute-start(bf16[256,2048]{1,0:T(8,128)(2,1)S(1)} %get-tuple-element.11), channel_id=1, source_target_pairs={{0,24},{1,25},{2,26},{3,27},{4,28},{5,29},{6,30},{7,31},{8,0},{9,1... | collective-permute-start | bytes 3145736 | tf_op jit(solution)/shard_map/ppermute | solution.py:240
  231.5 71.3 %collective-permute-start.32 = (bf16[256,2048]{1,0:T(8,128)(2,1)S(1)}, bf16[256,2048]{1,0:T(8,128)(2,1)S(1)}, u32[]{:S(2)}, u32[]{:S(2)}) collective-permute-start(bf16[256,2048]{1,0:T(8,128)(2,1)S(1)} %collective-permute-done.31.refs_3_.refs_4_), channel_id=1, source_target_pairs={{0,1},{1,0},{2,3},{3,2},{4,5},{5,4},{6,7},{7,6},{8,9},{9,8},{10,11... | collective-permute-start | bytes 3145736 | tf_op jit(solution)/shard_map/ppermute | solution.py:240
  231.5 137.4 %collective-permute-start.28 = (bf16[512,2048]{1,0:T(8,128)(2,1)}, bf16[512,2048]{1,0:T(8,128)(2,1)S(1)}, u32[]{:S(2)}, u32[]{:S(2)}) collective-permute-start(bf16[512,2048]{1,0:T(8,128)(2,1)} %collective-permute-done.27.refs_6_), channel_id=1, source_target_pairs={{0,1},{1,0},{2,3},{3,2},{4,5},{5,4},{6,7},{7,6},{8,9},{9,8},{10,11... | collective-permute-start | bytes 6291464 | tf_op jit(solution)/shard_map/ppermute | solution.py:240
  255.6 49.7 %collective-permute-start.34 = (bf16[256,2048]{1,0:T(8,128)(2,1)S(1)}, bf16[256,2048]{1,0:T(8,128)(2,1)S(1)}, u32[]{:S(2)}, u32[]{:S(2)}) collective-permute-start(bf16[256,2048]{1,0:T(8,128)(2,1)S(1)} %collective-permute-done.33.refs_5_.refs_6_), channel_id=1, source_target_pairs={{0,1},{1,0},{2,3},{3,2},{4,5},{5,4},{6,7},{7,6},{8,9},{9,8},{10,11... | collective-permute-start | bytes 3145736 | tf_op jit(solution)/shard_map/ppermute | solution.py:240
  302.2 46.0 %collective-permute-start.39 = (bf16[256,2048]{1,0:T(8,128)(2,1)S(1)}, bf16[256,2048]{1,0:T(8,128)(2,1)}, u32[]{:S(2)}, u32[]{:S(2)}) collective-permute-start(bf16[256,2048]{1,0:T(8,128)(2,1)S(1)} %collective-permute-done.37.refs_9_.refs_10_), channel_id=1, source_target_pairs={{0,4},{1,5},{2,6},{3,7},{4,0},{5,1},{6,2},{7,3},{8,12},{9,13},{10,... | collective-permute-start | bytes 3145736 | tf_op jit(solution)/shard_map/ppermute | solution.py:240
  303.7 65.1 %collective-permute-start.43 = (bf16[256,2048]{1,0:T(8,128)(2,1)S(1)}, bf16[256,2048]{1,0:T(8,128)(2,1)}, u32[]{:S(2)}, u32[]{:S(2)}) collective-permute-start(bf16[256,2048]{1,0:T(8,128)(2,1)S(1)} %collective-permute-done.41.refs_13_.refs_14_), channel_id=1, source_target_pairs={{0,4},{1,5},{2,6},{3,7},{4,0},{5,1},{6,2},{7,3},{8,12},{9,13},{10,... | collective-permute-start | bytes 3145736 | tf_op jit(solution)/shard_map/ppermute | solution.py:240
  306.3 70.3 %collective-permute-start.38 = (bf16[256,2048]{1,0:T(8,128)(2,1)S(1)}, bf16[256,2048]{1,0:T(8,128)(2,1)S(1)}, u32[]{:S(2)}, u32[]{:S(2)}) collective-permute-start(bf16[256,2048]{1,0:T(8,128)(2,1)S(1)} %collective-permute-done.37.refs_9_.refs_10_), channel_id=1, source_target_pairs={{0,1},{1,0},{2,3},{3,2},{4,5},{5,4},{6,7},{7,6},{8,9},{9,8},{10,11... | collective-permute-start | bytes 3145736 | tf_op jit(solution)/shard_map/ppermute | solution.py:240
  325.7 69.9 %collective-permute-start.42 = (bf16[256,2048]{1,0:T(8,128)(2,1)S(1)}, bf16[256,2048]{1,0:T(8,128)(2,1)S(1)}, u32[]{:S(2)}, u32[]{:S(2)}) collective-permute-start(bf16[256,2048]{1,0:T(8,128)(2,1)S(1)} %collective-permute-done.41.refs_13_.refs_14_), channel_id=1, source_target_pairs={{0,1},{1,0},{2,3},{3,2},{4,5},{5,4},{6,7},{7,6},{8,9},{9,8},{10,11... | collective-permute-start | bytes 3145736 | tf_op jit(solution)/shard_map/ppermute | solution.py:240
  348.2 49.1 %collective-permute-start.36 = (bf16[256,2048]{1,0:T(8,128)(2,1)S(1)}, bf16[256,2048]{1,0:T(8,128)(2,1)S(1)}, u32[]{:S(2)}, u32[]{:S(2)}) collective-permute-start(bf16[256,2048]{1,0:T(8,128)(2,1)S(1)} %collective-permute-done.35.refs_7_.refs_8_), channel_id=1, source_target_pairs={{0,1},{1,0},{2,3},{3,2},{4,5},{5,4},{6,7},{7,6},{8,9},{9,8},{10,11... | collective-permute-start | bytes 3145736 | tf_op jit(solution)/shard_map/ppermute | solution.py:240
  377.6 36.7 %collective-permute-start.49 = (bf16[192,2048]{1,0:T(8,128)(2,1)}, bf16[192,2048]{1,0:T(8,128)(2,1)}, u32[]{:S(2)}, u32[]{:S(2)}) collective-permute-start(bf16[192,2048]{1,0:T(8,128)(2,1)} %get-tuple-element.8.refs_0_), channel_id=1, source_target_pairs={{0,10},{1,11},{2,8},{3,9},{4,14},{5,15},{6,12},{7,13},{8,2},{9,3},... | collective-permute-start | bytes 2359304 | tf_op jit(solution)/shard_map/ppermute | solution.py:240
  395.5 38.2 %collective-permute-start.45 = (bf16[192,2048]{1,0:T(8,128)(2,1)}, bf16[192,2048]{1,0:T(8,128)(2,1)}, u32[]{:S(2)}, u32[]{:S(2)}) collective-permute-start(bf16[192,2048]{1,0:T(8,128)(2,1)} %get-tuple-element.8.refs_0_), channel_id=1, source_target_pairs={{0,8},{1,9},{2,10},{3,11},{4,12},{5,13},{6,14},{7,15},{8,0},{9,1},... | collective-permute-start | bytes 2359304 | tf_op jit(solution)/shard_map/ppermute | solution.py:240
  398.3 35.4 %collective-permute-start.46 = (bf16[192,2048]{1,0:T(8,128)(2,1)}, bf16[192,2048]{1,0:T(8,128)(2,1)}, u32[]{:S(2)}, u32[]{:S(2)}) collective-permute-start(bf16[192,2048]{1,0:T(8,128)(2,1)} %get-tuple-element.8.refs_0_), channel_id=1, source_target_pairs={{0,2},{1,3},{2,0},{3,1},{4,6},{5,7},{6,4},{7,5},{8,10},{9,11},{10,... | collective-permute-start | bytes 2359304 | tf_op jit(solution)/shard_map/ppermute | solution.py:240
  (66 other events, 1323.4 us)
